TPU v7x, 32 devices: a whole 2x2x4 slice. The times are simulated.
32 devices in a mesh: ep: 16 (over z, y, core), tp: 2 (over x).
Axes of the slice: x: 2, y: 2, z: 4, core: 2. Of those that a mesh axis runs over, the one named last changes fastest.
Arguments:
- tokens: bfloat16 [256, 2048], P('ep'), may hold values from -6 to 6
- recur_state: float32 [256, 8, 128, 128], P('ep', 'tp'), may hold values from -0.4 to 0.4
- attn_gain: float32 [2048], replicated, may hold values from 0.1 to 1.9
- query_weight: bfloat16 [2048, 1024], P(None, 'tp'), may hold values from -0.125 to 0.125
- key_weight: bfloat16 [2048, 1024], P(None, 'tp'), may hold values from -0.125 to 0.125
- value_weight: bfloat16 [2048, 1024], P(None, 'tp'), may hold values from -0.125 to 0.125
- outgate_weight: bfloat16 [2048, 1024], P(None, 'tp'), may hold values from -0.125 to 0.125
- beta_weight: bfloat16 [2048, 8], replicated, may hold values from -0.125 to 0.125
- decay_weight: bfloat16 [2048, 8], replicated, may hold values from -0.125 to 0.125
- decay_rate: float32 [8], replicated, may hold values from 0.05 to 2
- head_gain: float32 [128], replicated, may hold values from 0.1 to 1.9
- output_weight: bfloat16 [1024, 2048], P('tp'), may hold values from -0.1875 to 0.1875
- ffn_gain: float32 [2048], replicated, may hold values from 0.1 to 1.9
- routes: int32 [256, 2], P('ep'), may hold values from 0 to 3, all different within a row; in each aligned block of 16 rows (0 to 15, 16 to 31, ...) at most 16 rows name the same one
- route_weight: float32 [256, 2], P('ep'), may hold values from 0.2 to 1
- expert_gate: bfloat16 [16, 2048, 1024], P('ep', None, 'tp'), may hold values from -0.125 to 0.125
- expert_up: bfloat16 [16, 2048, 1024], P('ep', None, 'tp'), may hold values from -0.125 to 0.125
- expert_down: bfloat16 [16, 1024, 2048], P('ep', 'tp'), may hold values from -0.09375 to 0.09375
Outputs:
- mixed: bfloat16 [256, 2048], P('ep', 'tp')
- new_state: float32 [256, 8, 128, 128], P('ep', 'tp')
Inputs may be any that keep to these rules, and one draw needn't show every extreme that they name: `routes`: each row names 2 different experts; in each aligned block of 16 rows no expert is named by more than 16 rows.
All inputs are finite; a program needn't handle non-finite values.
Results may differ from a plain program's by a relative error of at most 0.014.
Values may be sent and summed in bfloat16 or wider, within the bound.
A program may use at most 64 MiB of HBM per device.

v0:
```python
import jax
import jax.numpy as jnp
from jax import lax
from jax.sharding import PartitionSpec as P

EPS = 1e-06


def rms_scale(values, gain):
    return values * lax.rsqrt(jnp.mean(values * values, axis=-1, keepdims=True) + EPS) * gain


def unit_rows(values):
    return values * lax.rsqrt(jnp.sum(values * values, axis=-1, keepdims=True) + EPS)


def slot_targets(group_routes, experts, capacity):
    flat = group_routes.reshape(-1)
    onehot = (flat[:, None] == jnp.arange(experts, dtype=jnp.int32)[None, :]).astype(jnp.int32)
    running = jnp.cumsum(onehot, axis=0)
    position = jnp.sum(running * onehot, axis=1) - 1
    return (flat * capacity + position).reshape(group_routes.shape)


def local(
    tokens,
    recur_state,
    attn_gain,
    query_weight,
    key_weight,
    value_weight,
    outgate_weight,
    beta_weight,
    decay_weight,
    decay_rate,
    head_gain,
    output_weight,
    ffn_gain,
    routes,
    route_weight,
    expert_gate,
    expert_up,
    expert_down,
):
    f32 = jnp.float32
    bf16 = jnp.bfloat16
    highest = lax.Precision.HIGHEST
    seq_count, model_width = tokens.shape
    heads_here = recur_state.shape[1]
    head_size = recur_state.shape[2]
    groups = lax.axis_size("ep")
    lanes = lax.axis_size("tp")
    lane_index = lax.axis_index("tp")
    normed = rms_scale(tokens.astype(f32), attn_gain).astype(bf16)
    qproj = jnp.dot(normed, query_weight, preferred_element_type=f32).astype(bf16)
    kproj = jnp.dot(normed, key_weight, preferred_element_type=f32).astype(bf16)
    vproj = jnp.dot(normed, value_weight, preferred_element_type=f32).astype(bf16)
    zproj = jnp.dot(normed, outgate_weight, preferred_element_type=f32).astype(bf16)
    first_head = lane_index * heads_here
    own_beta = lax.dynamic_slice_in_dim(beta_weight, first_head, heads_here, 1)
    own_decay = lax.dynamic_slice_in_dim(decay_weight, first_head, heads_here, 1)
    own_rate = lax.dynamic_slice_in_dim(decay_rate, first_head, heads_here, 0)
    strength = jax.nn.sigmoid(jnp.dot(normed, own_beta, preferred_element_type=f32))
    fading = jnp.exp(
        -own_rate * jax.nn.softplus(jnp.dot(normed, own_decay, preferred_element_type=f32))
    )

    def split_heads(proj):
        return proj.astype(f32).reshape(seq_count, heads_here, head_size)

    query = unit_rows(jax.nn.silu(split_heads(qproj))) * head_size ** (-0.5)
    keyvec = unit_rows(jax.nn.silu(split_heads(kproj)))
    value = jax.nn.silu(split_heads(vproj))
    recall = jnp.einsum("thd,thde->the", keyvec, recur_state, precision=highest)
    written = (strength[..., None] * keyvec)[..., :, None] * (value - fading[..., None] * recall)[
        ..., None, :
    ]
    new_state = fading[..., None, None] * recur_state + written
    readout = jnp.einsum("thd,thde->the", query, new_state, precision=highest)
    headed = (
        (rms_scale(readout, head_gain) * jax.nn.silu(split_heads(zproj)))
        .reshape(seq_count, heads_here * head_size)
        .astype(bf16)
    )
    partial_out = jnp.dot(headed, output_weight, preferred_element_type=f32)
    branch = lax.psum(partial_out, "tp").astype(bf16)
    resid = (tokens.astype(f32) + branch.astype(f32)).astype(bf16)
    ffn_in = rms_scale(resid.astype(f32), ffn_gain).astype(bf16)
    top_count = routes.shape[1]
    experts = groups // 4
    capacity = min(seq_count, max(2, (2 * seq_count * top_count + experts - 1) // experts))
    quarter = model_width // lanes
    targets = slot_targets(routes, experts, capacity)
    slot_ids = jnp.arange(experts * capacity, dtype=jnp.int32)
    select = jnp.any(slot_ids[:, None, None] == targets[None, :, :], axis=-1).astype(bf16)
    gate_local = expert_gate[0]
    up_local = expert_up[0]
    down_local = expert_down[0]
    packed = jnp.dot(select, ffn_in, preferred_element_type=f32).astype(bf16)
    packed = packed.reshape(experts, 1, capacity, ffn_in.shape[1])
    packed = jnp.broadcast_to(packed, (experts, 4, capacity, ffn_in.shape[1]))
    arrived = lax.all_to_all(
        packed.reshape(groups, capacity, ffn_in.shape[1]),
        "ep",
        split_axis=0,
        concat_axis=0,
        tiled=True,
    ).reshape(groups * capacity, model_width)
    gated = jnp.dot(arrived, gate_local, preferred_element_type=f32)
    lifted = jnp.dot(arrived, up_local, preferred_element_type=f32)
    hidden = (jax.nn.silu(gated) * lifted).astype(bf16)
    slice_terms = jnp.dot(hidden, down_local, preferred_element_type=f32).reshape(
        groups, capacity, model_width
    )
    shares = lax.psum_scatter(slice_terms, "tp", scatter_dimension=2, tiled=True).astype(bf16)
    returned = lax.all_to_all(shares, "ep", split_axis=0, concat_axis=0, tiled=True)
    merged = (
        returned.astype(f32)
        .reshape(experts, 4, capacity, quarter)
        .sum(axis=1)
        .reshape(experts * capacity, quarter)
    )
    combine = jnp.zeros((seq_count, experts * capacity), f32)
    for choice_idx in range(top_count):
        match = (targets[:, choice_idx, None] == slot_ids[None, :]).astype(f32)
        combine = combine + route_weight[:, choice_idx, None] * match
    moe = jnp.dot(combine, merged, precision=highest)
    resid_own = lax.dynamic_slice_in_dim(resid, lane_index * quarter, quarter, 1)
    mixed = (resid_own.astype(f32) + moe).astype(bf16)
    return (mixed, new_state)


def solution(mesh):
    return jax.shard_map(
        local,
        mesh=mesh,
        in_specs=(
            P("ep", None),
            P("ep", "tp", None, None),
            P(),
            P(None, "tp"),
            P(None, "tp"),
            P(None, "tp"),
            P(None, "tp"),
            P(),
            P(),
            P(),
            P(),
            P("tp", None),
            P(),
            P("ep", None),
            P("ep", None),
            P("ep", None, "tp"),
            P("ep", None, "tp"),
            P("ep", "tp", None),
        ),
        out_specs=(P("ep", "tp"), P("ep", "tp", None, None)),
        check_vma=False,
    )
```

profile of v0, /device:TPU:0, one launch (start us, length us, event | category | flops | bytes accessed | tf_op | source)
XLA Modules:
  0.0 138.9 jit_solution(11278963235603328612)
XLA Ops:
  7.3 1.1 fusion.23
  8.4 1.1 fusion.19
  9.5 2.1 %fusion.15 = f32[16,512]{1,0:T(8,128)S(1)} fusion(bf16[2048,512]{1,0:T(8,128)(2,1)} %param.22, bf16[16,2048]{1,0:T(8,128)(2,1)} %param.18, f32[2048]{0:T(1024)} %param.20, f32[16]{0:T(128)S(1)} %add_rsqrt_fusion.4), kind=kOutput, calls=%fused_computation.17 | convolution fusion | flops 33701888 | bytes 2203712 | tf_op jit(solution)/shard_map/dot_general | solution.py:56
  11.9 0.2 fusion.50
  12.2 2.0 %fusion.14 = f32[16,512]{1,0:T(8,128)S(1)} fusion(bf16[2048,512]{1,0:T(8,128)(2,1)} %param.23, bf16[16,2048]{1,0:T(8,128)(2,1)S(1)} %copy-done.3, f32[2048]{0:T(1024)S(1)} %copy-done.5, f32[16]{0:T(128)S(1)} %add_rsqrt_fusion.4), kind=kOutput, calls=%fused_computation.15 | convolution fusion | flops 33701888 | bytes 2203712 | tf_op jit(solution)/shard_map/dot_general | solution.py:57
  14.2 2.0 %fusion.16 = f32[16,512]{1,0:T(8,128)S(1)} fusion(bf16[2048,512]{1,0:T(8,128)(2,1)} %param.21, bf16[16,2048]{1,0:T(8,128)(2,1)S(1)} %copy-done.3, f32[2048]{0:T(1024)S(1)} %copy-done.5, f32[16]{0:T(128)S(1)} %add_rsqrt_fusion.4), kind=kOutput, calls=%fused_computation.19 | convolution fusion | flops 33701888 | bytes 2203712 | tf_op jit(solution)/shard_map/dot_general | solution.py:55
  16.6 5.5 %fusion.63 = f32[16,4,1,128]{3,2,1,0:T(1,128)S(1)} fusion(f32[16,4,128,1]{2,3,1,0:T(1,128)S(1)} %bitcast.66, f32[16,4,128,128]{3,2,1,0:T(8,128)} %param.19), kind=kOutput, calls=%fused_computation.91 | convolution fusion | flops 12582912 | bytes 4259840 | tf_op jit(solution)/shard_map/thd,thde->the/dot_general | solution.py:74
  22.2 1.5 %multiply_add_fusion = f32[16,4,128,128]{3,2,1,0:T(8,128)S(1)} fusion(f32[16,4,128,128]{3,2,1,0:T(8,128)S(1)} %copy-done.1, f32[16,4,128]{2,1,0:T(4,128)S(1)} %fusion.30, f32[16,4,128]{2,1,0:T(4,128)S(1)} %get-tuple-element.4, f32[16,4]{1,0:T(8,128)S(1)} %copy.39), kind=kLoop, calls=%fused_computation | loop fusion | flops 3145728 | bytes 8454400 | tf_op jit(solution)/shard_map/add | solution.py:78
  23.7 3.7 %fusion.64 = f32[16,4,1,128]{3,2,1,0:T(1,128)S(1)} fusion(f32[16,4,128,1]{2,3,1,0:T(1,128)S(1)} %bitcast.67, f32[16,4,128,128]{3,2,1,0:T(8,128)S(1)} %multiply_add_fusion), kind=kOutput, calls=%fused_computation.92 | convolution fusion | flops 12582912 | bytes 4259840 | tf_op jit(solution)/shard_map/thd,thde->the/dot_general | solution.py:79
  27.5 0.4 fusion.13
  28.1 2.0 %fusion.33 = f32[16,2048]{1,0:T(8,128)S(1)} fusion(bf16[512,2048]{1,0:T(8,128)(2,1)} %param.29, bf16[2,8,4,128]{3,2,1,0:T(4,128)(2,1)S(1)} %bitcast.69), kind=kOutput, calls=%fused_computation.50 | convolution fusion | flops 33554432 | bytes 2244608 | tf_op jit(solution)/shard_map/dot_general | solution.py:85
  30.1 11.3 %all-reduce.1 = bf16[16,2048]{1,0:T(8,128)(2,1)S(1)} all-reduce(f32[16,2048]{1,0:T(8,128)S(1)} %fusion.33), channel_id=1, replica_groups=mesh['ep'=16,'tp'=2] {'tp'}, use_global_device_ids=true, to_apply=%region_4.5 | all-reduce | flops 32768 | bytes 196608 | tf_op jit(solution)/shard_map/psum | solution.py:86
  41.9 0.2 select_reduce_fusion
  42.4 0.3 convolution_convert_fusion
  42.8 30.4 %all_to_all.10 = bf16[16,16,2048]{2,1,0:T(8,128)(2,1)S(1)} all-to-all(bf16[16,16,2048]{2,1,0:T(8,128)(2,1)S(1)} %bitcast.58), channel_id=1, replica_groups=mesh['ep'=16,'tp'=2] {'ep'}, dimensions={0} | all-to-all | bytes 2097152 | tf_op jit(solution)/shard_map/all_to_all | solution.py:102
  73.2 0.7 fusion.4
  73.9 0.9 copy-done.11
  74.7 0.7 fusion.9
  75.5 2.1 %fusion = f32[16,16,2048]{2,1,0:T(8,128)} fusion(bf16[16,16,512]{2,1,0:T(8,128)(2,1)S(1)} %bitcast.65, bf16[1,512,2048]{2,1,0:T(8,128)(2,1)S(1)} %copy-done), kind=kOutput, calls=%fused_computation.2 | convolution fusion | flops 536870912 | bytes 4456448 | tf_op jit(solution)/shard_map/dot_general | solution.py:112
  77.6 31.5 %reduce-scatter.2.cloned.1.call-done = f32[16,16,1024]{2,1,0:T(8,128)} async-done(((f32[16,16,2048]{2,1,0:T(8,128)}), f32[16,16,1024]{2,1,0:T(8,128)}) %reduce-scatter.2.cloned.1.call-update) | async-done | bytes 1048592 | tf_op jit(solution)/shard_map/reduce_scatter | solution.py:115
  109.1 2.1 %convert_element_type.83 = bf16[16,16,1024]{2,1,0:T(8,128)(2,1)} convert(f32[16,16,1024]{2,1,0:T(8,128)} %reduce-scatter.2.cloned.1.call-done) | non-fusion elementwise | flops 262144 | bytes 1572864 | tf_op jit(solution)/shard_map/convert_element_type | solution.py:115
  111.2 5.6 %all-to-all-start.1 = ((bf16[16,16,1024]{2,1,0:T(8,128)(2,1)}), bf16[16,16,1024]{2,1,0:T(8,128)(2,1)S(1)}, u32[]{:S(2)}, u32[]{:S(2)}) async-start(bf16[16,16,1024]{2,1,0:T(8,128)(2,1)} %convert_element_type.83), calls=%async_computation.2 | async-start | bytes 1048576 | tf_op jit(solution)/shard_map/all_to_all | solution.py:116
  116.8 14.2 %all-to-all-done.1 = bf16[16,16,1024]{2,1,0:T(8,128)(2,1)S(1)} async-done(((bf16[16,16,1024]{2,1,0:T(8,128)(2,1)}), bf16[16,16,1024]{2,1,0:T(8,128)(2,1)S(1)}, u32[]{:S(2)}, u32[]{:S(2)}) %all-to-all-start.1) | async-done | bytes 524320 | tf_op jit(solution)/shard_map/all_to_all | solution.py:116
  131.1 0.9 fusion.12
  (62 shorter events, 2.1 us)
Async XLA Ops:
  7.2 68.3 %copy-start = (bf16[1,512,2048]{2,1,0:T(8,128)(2,1)S(1)}, bf16[1,512,2048]{2,1,0:T(8,128)(2,1)}, u32[]{:S(2)}) copy-start(bf16[1,512,2048]{2,1,0:T(8,128)(2,1)} %param.35) | copy-start | bytes 6291460
  7.2 4.7 %copy-start.3 = (bf16[16,2048]{1,0:T(8,128)(2,1)S(1)}, bf16[16,2048]{1,0:T(8,128)(2,1)}, u32[]{:S(2)}) copy-start(bf16[16,2048]{1,0:T(8,128)(2,1)} %param.18) | copy-start | bytes 196612
  7.2 4.7 %copy-start.5 = (f32[2048]{0:T(1024)S(1)}, f32[2048]{0:T(1024)}, u32[]{:S(2)}) copy-start(f32[2048]{0:T(1024)} %param.20) | copy-start | bytes 24580
  7.2 4.6 %copy-start.13 = (f32[8]{0:T(128)S(1)}, f32[8]{0:T(128)}, u32[]{:S(2)}) copy-start(f32[8]{0:T(128)} %param.27) | copy-start | bytes 100
  7.2 4.7 %copy-start.12 = (bf16[2048,8]{0,1:T(8,128)(2,1)S(1)}, bf16[2048,8]{0,1:T(8,128)(2,1)}, u32[]{:S(2)}) copy-start(bf16[2048,8]{0,1:T(8,128)(2,1)} %param.26) | copy-start | bytes 98308
  7.2 101.8 %reduce-scatter.2.cloned.1.call-start = ((), (), s32[]{:S(2)}) async-start(), calls=%async_computation.3 | async-start | bytes 3145728 | tf_op jit(solution)/shard_map/reduce_scatter | solution.py:115
  16.6 5.6 %copy-start.1 = (f32[16,4,128,128]{3,2,1,0:T(8,128)S(1)}, f32[16,4,128,128]{3,2,1,0:T(8,128)}, u32[]{:S(2)}) copy-start(f32[16,4,128,128]{3,2,1,0:T(8,128)} %param.19) | copy-start | bytes 12582916
  23.7 3.7 %copy-start.2 = (f32[16,4,128,128]{3,2,1,0:T(8,128)}, f32[16,4,128,128]{3,2,1,0:T(8,128)S(1)}, u32[]{:S(2)}) copy-start(f32[16,4,128,128]{3,2,1,0:T(8,128)S(1)} %multiply_add_fusion) | copy-start | bytes 12582916
  23.7 3.8 %copy-start.4 = (bf16[2048,512]{1,0:T(8,128)(2,1)S(1)}, bf16[2048,512]{1,0:T(8,128)(2,1)}, u32[]{:S(2)}) copy-start(bf16[2048,512]{1,0:T(8,128)(2,1)} %param.24) | copy-start | bytes 6291460
  27.4 0.7 copy-start.9
  27.5 14.1 %copy-start.7 = (s32[16,2]{0,1:T(2,128)S(1)}, s32[16,2]{0,1:T(2,128)}, u32[]{:S(2)}) copy-start(s32[16,2]{0,1:T(2,128)} %param.31) | copy-start | bytes 388
  27.5 14.9 %copy-start.6 = (f32[2048]{0:T(1024)S(1)}, f32[2048]{0:T(1024)}, u32[]{:S(2)}) copy-start(f32[2048]{0:T(1024)} %param.30) | copy-start | bytes 24580
  42.3 30.9 %copy-start.10 = (bf16[1,2048,512]{2,1,0:T(8,128)(2,1)S(1)}, bf16[1,2048,512]{2,1,0:T(8,128)(2,1)}, u32[]{:S(2)}) copy-start(bf16[1,2048,512]{2,1,0:T(8,128)(2,1)} %param.33) | copy-start | bytes 6291460
  73.2 1.6 %copy-start.11 = (bf16[1,2048,512]{2,1,0:T(8,128)(2,1)S(1)}, bf16[1,2048,512]{2,1,0:T(8,128)(2,1)}, u32[]{:S(2)}) copy-start(bf16[1,2048,512]{2,1,0:T(8,128)(2,1)} %param.34) | copy-start | bytes 6291460
  77.5 39.3 %copy-start.8 = (f32[16,2]{0,1:T(2,128)S(1)}, f32[16,2]{0,1:T(2,128)}, u32[]{:S(2)}) copy-start(f32[16,2]{0,1:T(2,128)} %param.32) | copy-start | bytes 388
  111.2 19.9 %all-to-all-start.1 = ((bf16[16,16,1024]{2,1,0:T(8,128)(2,1)}), bf16[16,16,1024]{2,1,0:T(8,128)(2,1)S(1)}, u32[]{:S(2)}, u32[]{:S(2)}) async-start(bf16[16,16,1024]{2,1,0:T(8,128)(2,1)} %convert_element_type.83), calls=%async_computation.2 | async-start | bytes 1048576 | tf_op jit(solution)/shard_map/all_to_all | solution.py:116
Sparse Core Ops, SparseCore 0:
  77.7 31.3 reduce-scatter.1
where the time goes:
time: 139 us
  waiting for transfers between devices  45.8 us (33%)
  blocking collectives  41.7 us (30%)
  matrix products  23.6 us (17%)
  between operations  14.3 us (10%)
  other arithmetic  6.09 us (4%)
  starting transfers between devices  5.65 us (4%)
  local copies, waits for them, and re-layouts  1.71 us (1%)
    reduce_scatter x1, waiting for transfers between devices, local(): lax.psum_scatter(slice_terms, 'tp', scatter_dimension=2, tiled=True)  31.5 us
    all_to_all x1, blocking collectives, local(): lax.all_to_all(packed.reshape(groups, capacity, ffn_in.shape[1]), 'ep', s...  30.4 us
    all_to_all x1, waiting for transfers between devices, local(): lax.all_to_all(shares, 'ep', split_axis=0, concat_axis=0, tiled=True)  14.2 us
    psum x1, blocking collectives, local(): branch = lax.psum(partial_out, 'tp').astype(bf16)  11.3 us
    all_to_all x1, starting transfers between devices, local(): lax.all_to_all(shares, 'ep', split_axis=0, concat_axis=0, tiled=True)  5.61 us
    dot_general x1, matrix products, local(): recall = jnp.einsum('thd,thde->the', keyvec, recur_state, precision=highest)  5.48 us
    dot_general x1, matrix products, local(): readout = jnp.einsum('thd,thde->the', query, new_state, precision=highest)  3.66 us
  transfers between devices with their start and end apart: 2, of which 2 were waited for; matrix products, arithmetic and copies ran while one was open for 0% of the time, Pallas kernels for 0%

commit v1 on v0

--- a/solution.py
+++ b/solution.py
@@ -83,7 +83,7 @@
         .astype(bf16)
     )
     partial_out = jnp.dot(headed, output_weight, preferred_element_type=f32)
-    branch = lax.psum(partial_out, "tp").astype(bf16)
+    branch = jnp.sum(lax.all_gather(partial_out, "tp"), axis=0).astype(bf16)
     resid = (tokens.astype(f32) + branch.astype(f32)).astype(bf16)
     ffn_in = rms_scale(resid.astype(f32), ffn_gain).astype(bf16)
     top_count = routes.shape[1]

time: 139 us -> 137 us (0.986)
  blocking collectives: 41.7 us -> 37.9 us
    psum x1 -> x0, blocking collectives: 11.3 us -> none  [local(): branch = lax.psum(partial_out, 'tp').astype(bf16)]
    all_gather x0 -> x1, blocking collectives: none -> 7.11 us  [local(): branch = jnp.sum(lax.all_gather(partial_out, 'tp'), axis=0).astype(bf16)]
where the time goes in v1:
time: 137 us; the launch traced here: 136 us
  waiting for transfers between devices  46.7 us (34%)
  blocking collectives  37.9 us (28%)
  matrix products  23.6 us (17%)
  between operations  14.3 us (10%)
  other arithmetic  6.11 us (4%)
  starting transfers between devices  5.65 us (4%)
  local copies, waits for them, and re-layouts  1.73 us (1%)
    reduce_scatter x1, waiting for transfers between devices, local(): lax.psum_scatter(slice_terms, 'tp', scatter_dimension=2, tiled=True)  32.4 us
    all_to_all x1, blocking collectives, local(): lax.all_to_all(packed.reshape(groups, capacity, ffn_in.shape[1]), 'ep', s...  30.8 us
    all_to_all x1, waiting for transfers between devices, local(): lax.all_to_all(shares, 'ep', split_axis=0, concat_axis=0, tiled=True)  14.2 us
    all_gather x1, blocking collectives, local(): branch = jnp.sum(lax.all_gather(partial_out, 'tp'), axis=0).astype(bf16)  7.11 us
    all_to_all x1, starting transfers between devices, local(): lax.all_to_all(shares, 'ep', split_axis=0, concat_axis=0, tiled=True)  5.61 us
    dot_general x1, matrix products, local(): recall = jnp.einsum('thd,thde->the', keyvec, recur_state, precision=highest)  5.48 us
    dot_general x1, matrix products, local(): readout = jnp.einsum('thd,thde->the', query, new_state, precision=highest)  3.66 us
  transfers between devices with their start and end apart: 2, of which 2 were waited for; matrix products, arithmetic and copies ran while one was open for 0% of the time, Pallas kernels for 0%

profile of v1, /device:TPU:0, one launch (start us, length us, event | category | flops | bytes accessed | tf_op | source)
XLA Modules:
  0.0 136.0 jit_solution(8932454595161598915)
XLA Ops:
  7.3 1.1 fusion.23
  8.4 1.1 fusion.19
  9.5 2.1 %fusion.15 = f32[16,512]{1,0:T(8,128)S(1)} fusion(bf16[2048,512]{1,0:T(8,128)(2,1)} %param.22, bf16[16,2048]{1,0:T(8,128)(2,1)} %param.18, f32[2048]{0:T(1024)} %param.20, f32[16]{0:T(128)S(1)} %add_rsqrt_fusion.4), kind=kOutput, calls=%fused_computation.17 | convolution fusion | flops 33701888 | bytes 2203712 | tf_op jit(solution)/shard_map/dot_general | solution.py:56
  11.9 0.2 fusion.50
  12.2 2.0 %fusion.14 = f32[16,512]{1,0:T(8,128)S(1)} fusion(bf16[2048,512]{1,0:T(8,128)(2,1)} %param.23, bf16[16,2048]{1,0:T(8,128)(2,1)S(1)} %copy-done.3, f32[2048]{0:T(1024)S(1)} %copy-done.5, f32[16]{0:T(128)S(1)} %add_rsqrt_fusion.4), kind=kOutput, calls=%fused_computation.15 | convolution fusion | flops 33701888 | bytes 2203712 | tf_op jit(solution)/shard_map/dot_general | solution.py:57
  14.2 2.0 %fusion.16 = f32[16,512]{1,0:T(8,128)S(1)} fusion(bf16[2048,512]{1,0:T(8,128)(2,1)} %param.21, bf16[16,2048]{1,0:T(8,128)(2,1)S(1)} %copy-done.3, f32[2048]{0:T(1024)S(1)} %copy-done.5, f32[16]{0:T(128)S(1)} %add_rsqrt_fusion.4), kind=kOutput, calls=%fused_computation.19 | convolution fusion | flops 33701888 | bytes 2203712 | tf_op jit(solution)/shard_map/dot_general | solution.py:55
  16.6 5.5 %fusion.63 = f32[16,4,1,128]{3,2,1,0:T(1,128)S(1)} fusion(f32[16,4,128,1]{2,3,1,0:T(1,128)S(1)} %bitcast.68, f32[16,4,128,128]{3,2,1,0:T(8,128)} %param.19), kind=kOutput, calls=%fused_computation.91 | convolution fusion | flops 12582912 | bytes 4259840 | tf_op jit(solution)/shard_map/thd,thde->the/dot_general | solution.py:74
  22.2 1.5 %multiply_add_fusion = f32[16,4,128,128]{3,2,1,0:T(8,128)S(1)} fusion(f32[16,4,128,128]{3,2,1,0:T(8,128)S(1)} %copy-done.1, f32[16,4,128]{2,1,0:T(4,128)S(1)} %fusion.30, f32[16,4,128]{2,1,0:T(4,128)S(1)} %get-tuple-element.4, f32[16,4]{1,0:T(8,128)S(1)} %copy.39), kind=kLoop, calls=%fused_computation | loop fusion | flops 3145728 | bytes 8454400 | tf_op jit(solution)/shard_map/add | solution.py:78
  23.7 3.7 %fusion.64 = f32[16,4,1,128]{3,2,1,0:T(1,128)S(1)} fusion(f32[16,4,128,1]{2,3,1,0:T(1,128)S(1)} %bitcast.69, f32[16,4,128,128]{3,2,1,0:T(8,128)S(1)} %multiply_add_fusion), kind=kOutput, calls=%fused_computation.92 | convolution fusion | flops 12582912 | bytes 4259840 | tf_op jit(solution)/shard_map/thd,thde->the/dot_general | solution.py:79
  27.5 0.4 fusion.13
  28.1 2.0 %fusion.33 = f32[16,2048]{1,0:T(8,128)S(1)} fusion(bf16[512,2048]{1,0:T(8,128)(2,1)} %param.29, bf16[2,8,4,128]{3,2,1,0:T(4,128)(2,1)S(1)} %bitcast.71), kind=kOutput, calls=%fused_computation.50 | convolution fusion | flops 33554432 | bytes 2244608 | tf_op jit(solution)/shard_map/dot_general | solution.py:85
  30.1 7.1 %all-gather = f32[32,2048]{1,0:T(8,128)S(1)} all-gather(f32[16,2048]{1,0:T(8,128)S(1)} %fusion.33), channel_id=2, replica_groups=mesh['ep'=16,'tp'=2] {'tp'}, dimensions={0}, use_global_device_ids=true | all-gather | bytes 393216 | tf_op jit(solution)/shard_map/all_gather | solution.py:86
  37.7 0.2 select_reduce_fusion
  38.1 0.3 convolution_convert_fusion
  38.5 30.8 %all_to_all.10 = bf16[16,16,2048]{2,1,0:T(8,128)(2,1)S(1)} all-to-all(bf16[16,16,2048]{2,1,0:T(8,128)(2,1)S(1)} %bitcast.59), channel_id=1, replica_groups=mesh['ep'=16,'tp'=2] {'ep'}, dimensions={0} | all-to-all | bytes 2097152 | tf_op jit(solution)/shard_map/all_to_all | solution.py:102
  69.4 0.7 fusion.4
  70.1 0.9 copy-done.11
  71.0 0.7 fusion.9
  71.7 2.1 %fusion = f32[16,16,2048]{2,1,0:T(8,128)} fusion(bf16[16,16,512]{2,1,0:T(8,128)(2,1)S(1)} %bitcast.67, bf16[1,512,2048]{2,1,0:T(8,128)(2,1)S(1)} %copy-done), kind=kOutput, calls=%fused_computation.2 | convolution fusion | flops 536870912 | bytes 4456448 | tf_op jit(solution)/shard_map/dot_general | solution.py:112
  73.8 32.4 %reduce-scatter.2.cloned.1.call-done = f32[16,16,1024]{2,1,0:T(8,128)} async-done(((f32[16,16,2048]{2,1,0:T(8,128)}), f32[16,16,1024]{2,1,0:T(8,128)}) %reduce-scatter.2.cloned.1.call-update) | async-done | bytes 1048592 | tf_op jit(solution)/shard_map/reduce_scatter | solution.py:115
  106.2 2.1 %convert_element_type.83 = bf16[16,16,1024]{2,1,0:T(8,128)(2,1)} convert(f32[16,16,1024]{2,1,0:T(8,128)} %reduce-scatter.2.cloned.1.call-done) | non-fusion elementwise | flops 262144 | bytes 1572864 | tf_op jit(solution)/shard_map/convert_element_type | solution.py:115
  108.3 5.6 %all-to-all-start.1 = ((bf16[16,16,1024]{2,1,0:T(8,128)(2,1)}), bf16[16,16,1024]{2,1,0:T(8,128)(2,1)S(1)}, u32[]{:S(2)}, u32[]{:S(2)}) async-start(bf16[16,16,1024]{2,1,0:T(8,128)(2,1)} %convert_element_type.83), calls=%async_computation.2 | async-start | bytes 1048576 | tf_op jit(solution)/shard_map/all_to_all | solution.py:116
  113.9 14.2 %all-to-all-done.1 = bf16[16,16,1024]{2,1,0:T(8,128)(2,1)S(1)} async-done(((bf16[16,16,1024]{2,1,0:T(8,128)(2,1)}), bf16[16,16,1024]{2,1,0:T(8,128)(2,1)S(1)}, u32[]{:S(2)}, u32[]{:S(2)}) %all-to-all-start.1) | async-done | bytes 524320 | tf_op jit(solution)/shard_map/all_to_all | solution.py:116
  128.3 0.9 fusion.12
  (63 shorter events, 2.2 us)
Async XLA Ops:
  7.2 64.5 %copy-start = (bf16[1,512,2048]{2,1,0:T(8,128)(2,1)S(1)}, bf16[1,512,2048]{2,1,0:T(8,128)(2,1)}, u32[]{:S(2)}) copy-start(bf16[1,512,2048]{2,1,0:T(8,128)(2,1)} %param.35) | copy-start | bytes 6291460
  7.2 4.7 %copy-start.3 = (bf16[16,2048]{1,0:T(8,128)(2,1)S(1)}, bf16[16,2048]{1,0:T(8,128)(2,1)}, u32[]{:S(2)}) copy-start(bf16[16,2048]{1,0:T(8,128)(2,1)} %param.18) | copy-start | bytes 196612
  7.2 4.7 %copy-start.5 = (f32[2048]{0:T(1024)S(1)}, f32[2048]{0:T(1024)}, u32[]{:S(2)}) copy-start(f32[2048]{0:T(1024)} %param.20) | copy-start | bytes 24580
  7.2 4.6 %copy-start.13 = (f32[8]{0:T(128)S(1)}, f32[8]{0:T(128)}, u32[]{:S(2)}) copy-start(f32[8]{0:T(128)} %param.27) | copy-start | bytes 100
  7.2 4.7 %copy-start.12 = (bf16[2048,8]{0,1:T(8,128)(2,1)S(1)}, bf16[2048,8]{0,1:T(8,128)(2,1)}, u32[]{:S(2)}) copy-start(bf16[2048,8]{0,1:T(8,128)(2,1)} %param.26) | copy-start | bytes 98308
  7.2 99.0 %reduce-scatter.2.cloned.1.call-start = ((), (), s32[]{:S(2)}) async-start(), calls=%async_computation.3 | async-start | bytes 3145728 | tf_op jit(solution)/shard_map/reduce_scatter | solution.py:115
  16.6 5.6 %copy-start.1 = (f32[16,4,128,128]{3,2,1,0:T(8,128)S(1)}, f32[16,4,128,128]{3,2,1,0:T(8,128)}, u32[]{:S(2)}) copy-start(f32[16,4,128,128]{3,2,1,0:T(8,128)} %param.19) | copy-start | bytes 12582916
  23.7 3.7 %copy-start.2 = (f32[16,4,128,128]{3,2,1,0:T(8,128)}, f32[16,4,128,128]{3,2,1,0:T(8,128)S(1)}, u32[]{:S(2)}) copy-start(f32[16,4,128,128]{3,2,1,0:T(8,128)S(1)} %multiply_add_fusion) | copy-start | bytes 12582916
  23.7 3.8 %copy-start.4 = (bf16[2048,512]{1,0:T(8,128)(2,1)S(1)}, bf16[2048,512]{1,0:T(8,128)(2,1)}, u32[]{:S(2)}) copy-start(bf16[2048,512]{1,0:T(8,128)(2,1)} %param.24) | copy-start | bytes 6291460
  27.4 0.7 copy-start.9
  27.9 9.5 %copy-start.7 = (s32[16,2]{0,1:T(2,128)S(1)}, s32[16,2]{0,1:T(2,128)}, u32[]{:S(2)}) copy-start(s32[16,2]{0,1:T(2,128)} %param.31) | copy-start | bytes 388
  27.9 10.2 %copy-start.6 = (f32[2048]{0:T(1024)S(1)}, f32[2048]{0:T(1024)}, u32[]{:S(2)}) copy-start(f32[2048]{0:T(1024)} %param.30) | copy-start | bytes 24580
  38.0 31.3 %copy-start.10 = (bf16[1,2048,512]{2,1,0:T(8,128)(2,1)S(1)}, bf16[1,2048,512]{2,1,0:T(8,128)(2,1)}, u32[]{:S(2)}) copy-start(bf16[1,2048,512]{2,1,0:T(8,128)(2,1)} %param.33) | copy-start | bytes 6291460
  69.4 1.6 %copy-start.11 = (bf16[1,2048,512]{2,1,0:T(8,128)(2,1)S(1)}, bf16[1,2048,512]{2,1,0:T(8,128)(2,1)}, u32[]{:S(2)}) copy-start(bf16[1,2048,512]{2,1,0:T(8,128)(2,1)} %param.34) | copy-start | bytes 6291460
  73.8 40.2 %copy-start.8 = (f32[16,2]{0,1:T(2,128)S(1)}, f32[16,2]{0,1:T(2,128)}, u32[]{:S(2)}) copy-start(f32[16,2]{0,1:T(2,128)} %param.32) | copy-start | bytes 388
  108.3 19.9 %all-to-all-start.1 = ((bf16[16,16,1024]{2,1,0:T(8,128)(2,1)}), bf16[16,16,1024]{2,1,0:T(8,128)(2,1)S(1)}, u32[]{:S(2)}, u32[]{:S(2)}) async-start(bf16[16,16,1024]{2,1,0:T(8,128)(2,1)} %convert_element_type.83), calls=%async_computation.2 | async-start | bytes 1048576 | tf_op jit(solution)/shard_map/all_to_all | solution.py:116
Sparse Core Ops, SparseCore 0:
  73.9 32.2 reduce-scatter.1
